TPU v7x, 32 devices: a whole 2x2x4 slice. The times are simulated.
32 devices in a mesh: grp: 2 (over y), sp: 4 (over z), tp: 4 (over x, core).
Axes of the slice: x: 2, y: 2, z: 4, core: 2. Of those that a mesh axis runs over, the one named last changes fastest.
Arguments:
- stream: bfloat16 [2048, 4096], P(('grp', 'sp'), 'tp'), parts along dimension 0, may hold values from -6 to 6
- gain_pre: float32 [3, 4096], replicated, may hold values from 0.1 to 1.9
- w_in: bfloat16 [3, 4096, 1024], P(None, 'sp', 'tp'), may hold values from -0.09375 to 0.09375
- w_pool: bfloat16 [3, 4, 256, 256], P(None, 'tp'), may hold values from -0.375 to 0.375
- pool_scale: float32 [3, 1024], P(None, 'tp'), may hold values from 0.1 to 1.9
- w_out: bfloat16 [3, 1024, 4096], P(None, 'tp', 'sp'), may hold values from -0.5 to 0.5
- gain_post: float32 [3, 4096], replicated, may hold values from 0.1 to 1.9
Outputs:
- result: bfloat16 [2048, 4096], P(('grp', 'sp'), 'tp'), parts along dimension 0
There are 2 independent parts, one for each index of `grp`. A program takes and returns all parts, laid end to end along the dimension named above; an argument that names none is the same for every part. Nothing has to cross between parts.
All inputs are finite; a program needn't handle non-finite values.
Results may differ from a plain program's by a relative error of at most 0.02.
Values may be sent and summed in bfloat16 or wider, within the bound.
A program may use at most 64 MiB of HBM per device.

v0:
```python
import jax
import jax.numpy as jnp
from jax import lax
from jax.sharding import PartitionSpec as P

LAYERS = 3


WINDOWS = (2, 4, 8, 16)
EPS = 1e-06


def from_behind(block, axis, distance):
    devices = range(lax.axis_size(axis))
    route = [(i - distance, i) for i in devices if i - distance in devices]
    return lax.ppermute(block, axis, route)


def rms_scale(values, gain):
    inverse = lax.rsqrt(jnp.mean(values * values, axis=-1, keepdims=True) + EPS)
    return values * inverse * gain[None, :]


def per_device(stream, gain_pre, w_in, w_pool, pool_scale, w_out, gain_post):
    tok_rows = stream.shape[0]
    block_width = stream.shape[1]
    width = gain_pre.shape[1]
    group = w_pool.shape[2]
    reach = max(WINDOWS) - 1
    group_index = lax.axis_index("tp")
    window = jnp.where(
        group_index == 0, 2, jnp.where(group_index == 1, 4, jnp.where(group_index == 2, 8, 16))
    )
    positions = lax.axis_index("sp") * tok_rows + lax.iota(jnp.int32, tok_rows)
    count = jnp.minimum(positions + 1, window).astype(jnp.float32)
    gathered_in, gathered_out = (
        lax.all_gather(w_in, "sp", axis=1, tiled=True),
        lax.all_gather(w_out, "sp", axis=2, tiled=True),
    )
    current = stream
    feature_start = group_index * block_width
    for layer in range(LAYERS):
        full_rows = lax.all_gather(current, "tp", axis=1, tiled=True)
        normed = rms_scale(full_rows.astype(jnp.float32), gain_pre[layer]).astype(jnp.bfloat16)
        inner_sum = jnp.dot(normed, gathered_in[layer], preferred_element_type=jnp.float32)
        inner = inner_sum.astype(jnp.bfloat16)
        rim = from_behind(inner[tok_rows - reach :], "sp", 1)
        extended = jnp.concatenate([rim, inner], axis=0).astype(jnp.float32)
        summed = jnp.zeros((tok_rows, group), jnp.float32)
        for offset in range(max(WINDOWS)):
            window_slice = extended[reach - offset : reach - offset + tok_rows]
            summed = summed + jnp.where(offset < window, window_slice, 0.0)
        pooled = summed / count[:, None]
        spread = (pooled - inner.astype(jnp.float32)).astype(jnp.bfloat16)
        mixed = jnp.dot(spread, w_pool[layer, 0], preferred_element_type=jnp.float32)
        mixed = (mixed * pool_scale[layer][None, :]).astype(jnp.bfloat16)
        partial_value = jnp.dot(mixed, gathered_out[layer], preferred_element_type=jnp.float32)
        partial_value = partial_value.astype(jnp.bfloat16)
        branch = lax.psum_scatter(partial_value, "tp", scatter_dimension=1, tiled=True).astype(
            jnp.float32
        )
        squares = lax.psum(jnp.sum(branch * branch, axis=1), "tp")
        inverse = lax.rsqrt(squares / width + EPS)
        gain_block = lax.dynamic_slice_in_dim(gain_post[layer], feature_start, block_width, 0)
        normed_branch = branch * inverse[:, None] * gain_block[None, :]
        current = (current.astype(jnp.float32) + normed_branch).astype(jnp.bfloat16)
    return current


def solution(mesh):
    return jax.shard_map(
        per_device,
        mesh=mesh,
        in_specs=(
            P(("grp", "sp"), "tp"),
            P(),
            P(None, "sp", "tp"),
            P(None, "tp", None, None),
            P(None, "tp"),
            P(None, "tp", "sp"),
            P(),
        ),
        out_specs=P(("grp", "sp"), "tp"),
        check_vma=False,
    )
```

profile of v0, /device:TPU:0, one launch (start us, length us, event | category | flops | bytes accessed | tf_op | source)
XLA Modules:
  0.0 473.9 jit_solution(1717130798795279151)
XLA Ops:
  10.6 23.6 %all-gather.6.cloned.1.call-done = bf16[256,4096]{1,0:T(8,128)(2,1)} async-done(((bf16[256,1024]{1,0:T(8,128)(2,1)}), bf16[256,4096]{1,0:T(8,128)(2,1)}) %all-gather.6.cloned.1.call-update) | async-done | bytes 2097168 | tf_op jit(solution)/shard_map/all_gather | solution.py:43
  34.2 2.1 fusion
  36.3 114.8 %all-gather.8.cloned.1.call-done = bf16[3,4096,256]{2,1,0:T(8,128)(2,1)} async-done(((bf16[3,1024,256]{2,1,0:T(8,128)(2,1)}), bf16[3,4096,256]{2,1,0:T(8,128)(2,1)}) %all-gather.8.cloned.1.call-update) | async-done | bytes 6291472 | tf_op jit(solution)/shard_map/all_gather | solution.py:37
  151.1 3.0 fusion.24
  156.8 109.5 %all-gather.10.cloned.1.call-done = bf16[3,256,4096]{2,1,0:T(8,128)(2,1)} async-done(((bf16[3,256,1024]{2,1,0:T(8,128)(2,1)}), bf16[3,256,4096]{2,1,0:T(8,128)(2,1)}) %all-gather.10.cloned.1.call-update) | async-done | bytes 6291472 | tf_op jit(solution)/shard_map/all_gather | solution.py:38
  266.3 4.4 convolution_convert_fusion.2
  270.8 29.4 %reduce-scatter.4.cloned.1.call-done = bf16[256,1024]{1,0:T(8,128)(2,1)} async-done(((bf16[256,4096]{1,0:T(8,128)(2,1)}), bf16[256,1024]{1,0:T(8,128)(2,1)}) %reduce-scatter.4.cloned.1.call-update) | async-done | bytes 524304 | tf_op jit(solution)/shard_map/reduce_scatter | solution.py:59
  301.4 5.8 %psum.21 = f32[256]{0:T(256)S(1)} all-reduce(f32[256]{0:T(256)S(1)} %fusion.33), channel_id=1, replica_groups=mesh['grp'=2,'sp'=4,'tp'=4] {'tp'}, use_global_device_ids=true, to_apply=%region_3.4 | all-reduce | flops 256 | bytes 2048 | tf_op jit(solution)/shard_map/psum | solution.py:62
  307.2 2.1 fusion.36
  309.4 23.3 %all-gather.12.cloned.1.call-done = bf16[256,4096]{1,0:T(8,128)(2,1)} async-done(((bf16[256,1024]{1,0:T(8,128)(2,1)}), bf16[256,4096]{1,0:T(8,128)(2,1)}) %all-gather.12.cloned.1.call-update) | async-done | bytes 2097168 | tf_op jit(solution)/shard_map/all_gather | solution.py:43
  332.7 2.1 fusion.3
  334.7 3.0 fusion.27
  337.8 3.4 collective-permute-start.1
  342.5 4.4 convolution_convert_fusion.1
  347.0 32.0 %reduce-scatter.6.cloned.1.call-done = bf16[256,1024]{1,0:T(8,128)(2,1)} async-done(((bf16[256,4096]{1,0:T(8,128)(2,1)}), bf16[256,1024]{1,0:T(8,128)(2,1)}) %reduce-scatter.6.cloned.1.call-update) | async-done | bytes 524304 | tf_op jit(solution)/shard_map/reduce_scatter | solution.py:59
  380.3 5.8 %psum.22 = f32[256]{0:T(256)S(1)} all-reduce(f32[256]{0:T(256)S(1)} %fusion.37), channel_id=1, replica_groups=mesh['grp'=2,'sp'=4,'tp'=4] {'tp'}, use_global_device_ids=true, to_apply=%region_7.8 | all-reduce | flops 256 | bytes 2048 | tf_op jit(solution)/shard_map/psum | solution.py:62
  386.0 2.1 fusion.40
  388.2 23.3 %all-gather.14.cloned.1.call-done = bf16[256,4096]{1,0:T(8,128)(2,1)} async-done(((bf16[256,1024]{1,0:T(8,128)(2,1)}), bf16[256,4096]{1,0:T(8,128)(2,1)}) %all-gather.14.cloned.1.call-update) | async-done | bytes 2097168 | tf_op jit(solution)/shard_map/all_gather | solution.py:43
  413.6 3.0 fusion.30
  416.6 3.4 collective-permute-start.2
  421.4 4.3 convolution_convert_fusion
  425.8 32.1 %reduce-scatter.8.cloned.1.call-done = bf16[256,1024]{1,0:T(8,128)(2,1)} async-done(((bf16[256,4096]{1,0:T(8,128)(2,1)}), bf16[256,1024]{1,0:T(8,128)(2,1)}) %reduce-scatter.8.cloned.1.call-update) | async-done | bytes 524304 | tf_op jit(solution)/shard_map/reduce_scatter | solution.py:59
  459.1 5.8 %psum.23 = f32[256]{0:T(256)S(1)} all-reduce(f32[256]{0:T(256)S(1)} %fusion.41), channel_id=1, replica_groups=mesh['grp'=2,'sp'=4,'tp'=4] {'tp'}, use_global_device_ids=true, to_apply=%region_11.12 | all-reduce | flops 256 | bytes 2048 | tf_op jit(solution)/shard_map/psum | solution.py:62
  464.9 2.1 fusion.44
  (53 shorter events, 15.6 us)
Async XLA Ops:
  6.5 27.7 %all-gather.6.cloned.1.call-start = ((), (), s32[]{:S(2)}) async-start(), calls=%async_computation.3 | async-start | bytes 2621440 | tf_op jit(solution)/shard_map/all_gather | solution.py:43
  7.3 143.9 %all-gather.8.cloned.1.call-start = ((), (), s32[]{:S(2)}) async-start(), calls=%async_computation.4 | async-start | bytes 7864320 | tf_op jit(solution)/shard_map/all_gather | solution.py:37
  8.0 258.3 %all-gather.10.cloned.1.call-start = ((), (), s32[]{:S(2)}) async-start(), calls=%async_computation.5 | async-start | bytes 7864320 | tf_op jit(solution)/shard_map/all_gather | solution.py:38
  8.7 291.5 %reduce-scatter.4.cloned.1.call-start = ((), (), s32[]{:S(2)}) async-start(), calls=%async_computation.6 | async-start | bytes 2621440 | tf_op jit(solution)/shard_map/reduce_scatter | solution.py:59
  36.3 230.0 %copy-start.4 = (bf16[3,1,256,256]{3,2,1,0:T(8,128)(2,1)S(1)}, bf16[3,1,256,256]{3,2,1,0:T(8,128)(2,1)}, u32[]{:S(2)}) copy-start(bf16[3,1,256,256]{3,2,1,0:T(8,128)(2,1)} %param.10) | copy-start | bytes 1179652
  154.1 2.6 collective-permute-start
  266.3 4.4 copy-start.3
  266.3 40.9 %copy-start.2 = (bf16[256,1024]{1,0:T(8,128)(2,1)S(1)}, bf16[256,1024]{1,0:T(8,128)(2,1)}, u32[]{:S(2)}) copy-start(bf16[256,1024]{1,0:T(8,128)(2,1)} %param.7) | copy-start | bytes 1572868
  270.7 62.0 %all-gather.12.cloned.1.call-start = ((), (), s32[]{:S(2)}) async-start(), calls=%async_computation.7 | async-start | bytes 2621440 | tf_op jit(solution)/shard_map/all_gather | solution.py:43
  309.3 69.7 %reduce-scatter.6.cloned.1.call-start = ((), (), s32[]{:S(2)}) async-start(), calls=%async_computation.8 | async-start | bytes 2621440 | tf_op jit(solution)/shard_map/reduce_scatter | solution.py:59
  337.8 4.7 %collective-permute-start.1 = (bf16[15,256]{1,0:T(8,128)(2,1)S(1)}, bf16[15,256]{1,0:T(8,128)(2,1)S(1)}, u32[]{:S(2)}, u32[]{:S(2)}) collective-permute-start(bf16[15,256]{1,0:T(8,128)(2,1)S(1)} %slice.296), channel_id=1, source_target_pairs={{0,4},{4,8},{8,12},{1,5},{5,9},{9,13},{2,6},{6,10},{10,14},{3,7},{... | collective-permute-start | bytes 23048 | tf_op jit(solution)/shard_map/ppermute | solution.py:16
  342.5 43.5 %copy-start.1 = (bf16[256,1024]{1,0:T(8,128)(2,1)S(1)}, bf16[256,1024]{1,0:T(8,128)(2,1)}, u32[]{:S(2)}) copy-start(bf16[256,1024]{1,0:T(8,128)(2,1)} %fusion.36) | copy-start | bytes 1572868
  346.9 64.6 %all-gather.14.cloned.1.call-start = ((), (), s32[]{:S(2)}) async-start(), calls=%async_computation.9 | async-start | bytes 2621440 | tf_op jit(solution)/shard_map/all_gather | solution.py:43
  388.2 69.8 %reduce-scatter.8.cloned.1.call-start = ((), (), s32[]{:S(2)}) async-start(), calls=%async_computation.10 | async-start | bytes 2621440 | tf_op jit(solution)/shard_map/reduce_scatter | solution.py:59
  416.6 4.7 %collective-permute-start.2 = (bf16[15,256]{1,0:T(8,128)(2,1)S(1)}, bf16[15,256]{1,0:T(8,128)(2,1)S(1)}, u32[]{:S(2)}, u32[]{:S(2)}) collective-permute-start(bf16[15,256]{1,0:T(8,128)(2,1)S(1)} %slice.315), channel_id=1, source_target_pairs={{0,4},{4,8},{8,12},{1,5},{5,9},{9,13},{2,6},{6,10},{10,14},{3,7},{... | collective-permute-start | bytes 23048 | tf_op jit(solution)/shard_map/ppermute | solution.py:16
  421.4 43.5 %copy-start = (bf16[256,1024]{1,0:T(8,128)(2,1)S(1)}, bf16[256,1024]{1,0:T(8,128)(2,1)}, u32[]{:S(2)}) copy-start(bf16[256,1024]{1,0:T(8,128)(2,1)} %fusion.40) | copy-start | bytes 1572868
Sparse Core Ops, SparseCore 0:
  8.9 25.2 all-gather.5
  35.8 115.3 all-gather.7
  152.7 113.5 all-gather.9
  270.8 29.3 reduce-scatter.3
  309.4 23.1 all-gather.11
  347.1 31.9 reduce-scatter.5
  388.3 23.1 all-gather.13
  425.9 31.9 reduce-scatter.7
where the time goes:
time: 475 us; the launch traced here: 474 us
  waiting for transfers between devices  394 us (83%)
  matrix products  22 us (5%)
  blocking collectives  17.3 us (4%)
  other arithmetic  16.3 us (3%)
  between operations  13.7 us (3%)
  starting transfers between devices  8.35 us (2%)
    all_gather x1, waiting for transfers between devices, per_device(): lax.all_gather(w_in, 'sp', axis=1, tiled=True)  115 us
    all_gather x1, waiting for transfers between devices, per_device(): lax.all_gather(w_out, 'sp', axis=2, tiled=True)  109 us
    reduce_scatter x3, waiting for transfers between devices, per_device(): lax.psum_scatter(partial_value, 'tp', scatter_dimension=1, tiled=True)  93.6 us
    all_gather x3, waiting for transfers between devices, per_device(): full_rows = lax.all_gather(current, 'tp', axis=1, tiled=True)  70.2 us
    psum x3, blocking collectives, per_device(): squares = lax.psum(jnp.sum(branch * branch, axis=1), 'tp')  17.3 us
    dot_general x3, matrix products, per_device(): jnp.dot(mixed, gathered_out[layer], preferred_element_type=jnp.float32)  13.1 us
  transfers between devices with their start and end apart: 11, of which 11 were waited for; matrix products, arithmetic and copies ran while one was open for 1% of the time, Pallas kernels for 0%

commit v1 on v0

v1 whole, which is shorter than its diff:
```python
import functools

import jax
import jax.numpy as jnp
from jax import lax
from jax.experimental import pallas as pl
from jax.experimental.pallas import tpu as pltpu
from jax.sharding import PartitionSpec as P

EPS = 1e-06
HALO = 16
CHUNKS = 4
MESH = pl.DeviceIdType.MESH
F32 = jnp.float32
BF16 = jnp.bfloat16


def kernel(
    G, S, T, layers, width,
    stream, gain_pre, w_in, w_pool, pool_scale, w_out, gain_post,
    out,
    win, wout, ag, part, pair, summed, xgot, normed, acc, ss, branch, ext, halo, sq,
    load_sem, zs_sem, zr_sem, ys_sem, yr_sem,
    agp_sem, agx_sem, agr_sem, ps_sem, pr_sem, xs_sem, xr_sem, qs_sem, qr_sem, hs_sem, hr_sem,
):
    g, s, t = lax.axis_index("grp"), lax.axis_index("sp"), lax.axis_index("tp")
    pairs = T // 2
    p, c = lax.div(t, 2), lax.rem(t, 2)
    mate = p * 2 + 1 - c
    R, F = stream.shape
    group = w_pool.shape[2]
    rows_in, cols_out = w_in.shape[1], w_out.shape[2]
    per = S // T
    step_rows = R // CHUNKS
    use_y = G == 2

    def remote(src, dst, send, recv, where):
        return pltpu.make_async_remote_copy(
            src_ref=src, dst_ref=dst, send_sem=send, recv_sem=recv,
            device_id=where, device_id_type=MESH,
        )

    def span(m, src, which):
        size = rows_in if m % 2 == 0 else group
        small, big = size * 3 // 8, size * 5 // 8
        if not use_y:
            start, length = 0, size
        elif which == "z":
            start, length = g * small, big
        else:
            start, length = g * big, small
        if m % 2 == 0:
            return win.at[m // 2, pl.ds(pl.multiple_of(src * size + start, 16), length), :]
        return wout.at[m // 2, src, pl.ds(pl.multiple_of(start, 16), length), :]

    def z_copy(m, src, way):
        view = span(m, src, "z")
        to = s + 1 if way == 0 else s - 1
        return remote(view, view, zs_sem.at[m, src, way], zr_sem.at[m, src], {"sp": to})

    def y_copy(m, src):
        view = span(m, src, "y")
        return remote(view, view, ys_sem.at[m, src], yr_sem.at[m, src], {"grp": 1 - g})

    def load(m):
        if m % 2 == 0:
            return pltpu.make_async_copy(
                w_in.at[m // 2],
                win.at[m // 2, pl.ds(pl.multiple_of(s * rows_in, 16), rows_in), :],
                load_sem.at[m],
            )
        return pltpu.make_async_copy(w_out.at[m // 2], wout.at[m // 2, s], load_sem.at[m])

    M = 2 * layers

    def own(m):
        if m < M:
            load(m).wait()
            pl.when(s < S - 1)(lambda: z_copy(m, s, 0).start())
            pl.when(s > 0)(lambda: z_copy(m, s, 1).start())

    def relay(m, k):
        def from_left():
            src = s - 1 - k
            z_copy(m, src, 0).wait_recv()
            pl.when(s < S - 1)(lambda: z_copy(m, src, 0).start())
            if use_y:
                y_copy(m, src).start()

        def from_right():
            src = s + 1 + k
            z_copy(m, src, 1).wait_recv()
            pl.when(s > 0)(lambda: z_copy(m, src, 1).start())
            if use_y:
                y_copy(m, src).start()

        pl.when(s - 1 - k >= 0)(from_left)
        pl.when(s + 1 + k <= S - 1)(from_right)

    def pump(m):
        for k in range(S - 1):
            relay(m, k)
            if k == 0:
                own(m + 1)

    def finish(m):
        if use_y:
            for src in range(S):
                pl.when(s != src)(lambda: y_copy(m, src).wait_recv())

    def ag_copy(l, block, j, sem, to):
        view = ag.at[l, block, pl.ds(j * step_rows, step_rows), :]
        return remote(view, view, sem, agr_sem.at[l, block, j], {"tp": to})

    def ag_start(l):
        for j in range(CHUNKS):
            for d in range(1, pairs):
                q = lax.rem(p + d, pairs)
                ag_copy(l, t, j, agx_sem.at[l, q, j], q * 2 + c).start()
        for j in range(CHUNKS):
            ag_copy(l, t, j, agp_sem.at[l, p, j], mate).start()

    def absorb(l, block, first):
        def body(i, carry):
            rows = pl.ds(pl.multiple_of(i * 32, 32), 32)
            x = ag[l, block, rows, :].astype(F32)
            gain = gain_pre[pl.ds(l, 1), pl.ds(pl.multiple_of(block * F, 128), F)]
            square = jnp.broadcast_to(jnp.sum(x * x, axis=1, keepdims=True), (32, 128))
            ss[rows, :] = square if first else ss[rows, :] + square
            normed[rows, :] = (x * gain).astype(BF16)
            return carry

        lax.fori_loop(0, R // 32, body, 0)
        product = jnp.dot(
            normed[...], win[l, pl.ds(pl.multiple_of(block * F, 128), F), :],
            preferred_element_type=F32,
        )
        acc[...] = product if first else acc[...] + product

    def ag_wait(l, block):
        for j in range(CHUNKS):
            ag_copy(l, block, j, agp_sem.at[l, p, j], mate).wait_recv()

    def ag_relay(l):
        for d in range(1, pairs):
            q = lax.rem(p + d, pairs)
            for j in range(CHUNKS):
                copy = ag_copy(l, q * 2 + c, j, agp_sem.at[l, q, j], mate)
                copy.wait_recv()
                copy.start()

    def halo_copy(l):
        return remote(
            ext.at[l, pl.ds(R, HALO), :], halo.at[l], hs_sem.at[l], hr_sem.at[l], {"sp": s + 1}
        )

    def pair_copy(l, q, j):
        rows = pl.ds(j * step_rows, step_rows)
        return remote(
            part.at[l, q * 2 + 1 - c, rows, :], pair.at[l, q, rows, :],
            ps_sem.at[l, q, j], pr_sem.at[l, q, j], {"tp": mate},
        )

    def cross_copy(l, q, j):
        rows = pl.ds(j * step_rows, step_rows)
        return remote(
            summed.at[l, q, rows, :], xgot.at[l, p, rows, :],
            xs_sem.at[l, q, j], xr_sem.at[l, p, j], {"tp": q * 2 + c},
        )

    def cross_wait(l, q, j):
        rows = pl.ds(j * step_rows, step_rows)
        remote(
            summed.at[l, q, rows, :], xgot.at[l, q, rows, :],
            xs_sem.at[l, q, j], xr_sem.at[l, q, j], {"tp": q * 2 + c},
        ).wait_recv()

    def sq_copy(l, slot, to):
        return remote(sq.at[l, slot], sq.at[l, slot], qs_sem.at[l, to], qr_sem.at[l, slot], {"tp": to})

    for m in range(M):
        load(m).start()
    barrier = pltpu.get_barrier_semaphore()

    def greet(where):
        pl.semaphore_signal(barrier, inc=1, device_id=where, device_id_type=MESH)

    pl.when(s < S - 1)(lambda: greet({"sp": s + 1}))
    pl.when(s > 0)(lambda: greet({"sp": s - 1}))
    if use_y:
        greet({"grp": 1 - g})
    for d in range(1, T):
        greet({"tp": lax.rem(t + d, T)})
    ag[0, t] = stream[...]
    ends = jnp.where(s > 0, 1, 0) + jnp.where(s < S - 1, 1, 0)
    pl.semaphore_wait(barrier, ends + (1 if use_y else 0) + T - 1)

    own(0)
    for l in range(layers):
        ag_start(l)
        if l == 0:
            pump(0)
            finish(0)
        else:
            pump(2 * l + 1)
        ag_relay(l)
        if l > 0:
            finish(2 * l)
        absorb(l, t, True)
        ag_wait(l, mate)
        absorb(l, mate, False)
        for d in range(1, pairs):
            q = lax.rem(p + d, pairs)
            absorb(l, q * 2 + c, False)
            ag_wait(l, q * 2 + 1 - c)
            absorb(l, q * 2 + 1 - c, False)
        inverse = lax.rsqrt(ss[:, 0:1] / width + EPS)
        ext[l, pl.ds(HALO, R), :] = (acc[...] * inverse).astype(BF16)
        pl.when(s < S - 1)(lambda: halo_copy(l).start())
        if l == 0:
            pump(1)
        pl.when(s > 0)(lambda: halo_copy(l).wait_recv())

        @pl.when(s == 0)
        def _():
            ext[l, pl.ds(0, HALO), :] = jnp.zeros((HALO, group), BF16)

        @pl.when(s > 0)
        def _():
            ext[l, pl.ds(0, HALO), :] = halo[l]

        values = ext[l].astype(F32)
        two = values + pltpu.roll(values, 1, 0)
        four = two + pltpu.roll(two, 2, 0)
        eight = four + pltpu.roll(four, 4, 0)
        sixteen = eight + pltpu.roll(eight, 8, 0)
        total = jnp.where(t == 0, two, jnp.where(t == 1, four, jnp.where(t == 2, eight, sixteen)))
        window = jnp.where(t == 0, 2, jnp.where(t == 1, 4, jnp.where(t == 2, 8, 16)))
        place = s * R + lax.broadcasted_iota(jnp.int32, (R, group), 0)
        count = jnp.minimum(place + 1, window).astype(F32)
        spread = (total[HALO:, :] / count - values[HALO:, :]).astype(BF16)
        mixed = jnp.dot(spread, w_pool[l, 0], preferred_element_type=F32)
        mixed = (mixed * pool_scale[l : l + 1, :]).astype(BF16)
        finish(2 * l + 1)

        def project(dest):
            for k in range(per):
                value = jnp.dot(mixed, wout[l, dest * per + k], preferred_element_type=F32)
                part[l, dest, :, k * cols_out : (k + 1) * cols_out] = value.astype(BF16)

        for d in range(1, pairs):
            q = lax.rem(p + d, pairs)
            project(q * 2 + 1 - c)
            for j in range(CHUNKS):
                pair_copy(l, q, j).start()
        for d in range(1, pairs):
            q = lax.rem(p + d, pairs)
            project(q * 2 + c)
            for j in range(CHUNKS):
                rows = pl.ds(j * step_rows, step_rows)
                pair_copy(l, q, j).wait_recv()
                summed[l, q, rows, :] = (
                    part[l, q * 2 + c, rows, :].astype(F32) + pair[l, q, rows, :].astype(F32)
                ).astype(BF16)
                cross_copy(l, q, j).start()
        project(mate)
        for j in range(CHUNKS):
            pair_copy(l, p, j).start()
        project(t)
        if l + 1 < layers:
            pump(2 * l + 2)
        for j in range(CHUNKS):
            rows = pl.ds(j * step_rows, step_rows)
            pair_copy(l, p, j).wait_recv()
            for d in range(1, pairs):
                cross_wait(l, lax.rem(p + d, pairs), j)

            def add(i, carry):
                rows = pl.ds(pl.multiple_of(j * step_rows + i * 32, 32), 32)
                value = part[l, t, rows, :].astype(F32) + pair[l, p, rows, :].astype(F32)
                for d in range(1, pairs):
                    value = value + xgot[l, lax.rem(p + d, pairs), rows, :].astype(F32)
                branch[rows, :] = value
                ss[rows, :] = jnp.broadcast_to(jnp.sum(value * value, axis=1, keepdims=True), (32, 128))
                return carry

            lax.fori_loop(0, step_rows // 32, add, 0)
        sq[l, t] = jnp.transpose(ss[...])[0:8, :]
        for d in range(1, T):
            sq_copy(l, t, lax.rem(t + d, T)).start()
        for d in range(1, T):
            other = lax.rem(t + d, T)
            sq_copy(l, other, other).wait_recv()
        squares = sq[l, 0]
        for k in range(1, T):
            squares = squares + sq[l, k]
        inverse = lax.rsqrt(squares / width + EPS)
        ss[...] = jnp.transpose(jnp.concatenate([inverse] * 16, axis=0))

        def update(i, carry):
            rows = pl.ds(pl.multiple_of(i * 32, 32), 32)
            gain = gain_post[pl.ds(l, 1), pl.ds(pl.multiple_of(t * F, 128), F)]
            value = ag[l, t, rows, :].astype(F32) + branch[rows, :] * ss[rows, 0:1] * gain
            if l + 1 < layers:
                ag[l + 1, t, rows, :] = value.astype(BF16)
            else:
                out[rows, :] = value.astype(BF16)
            return carry

        lax.fori_loop(0, R // 32, update, 0)

    for l in range(layers):
        pl.when(s < S - 1)(lambda: halo_copy(l).wait_send())
        for d in range(1, T):
            sq_copy(l, t, lax.rem(t + d, T)).wait_send()
        for j in range(CHUNKS):
            for q in range(pairs):
                ag_copy(l, t, j, agp_sem.at[l, q, j], mate).wait_send()
                pair_copy(l, q, j).wait_send()
            for d in range(1, pairs):
                q = lax.rem(p + d, pairs)
                ag_copy(l, t, j, agx_sem.at[l, q, j], mate).wait_send()
                cross_copy(l, q, j).wait_send()
    for m in range(M):
        for src in range(S):
            pl.when(jnp.logical_and(src <= s, s < S - 1))(lambda: z_copy(m, src, 0).wait_send())
            pl.when(jnp.logical_and(src >= s, s > 0))(lambda: z_copy(m, src, 1).wait_send())
            if use_y:
                pl.when(s != src)(lambda: y_copy(m, src).wait_send())


def per_device(G, S, T, stream, gain_pre, w_in, w_pool, pool_scale, w_out, gain_post):
    layers, width = gain_pre.shape
    R, F = stream.shape
    group = w_pool.shape[2]
    pairs = T // 2
    M = 2 * layers
    dma = pltpu.SemaphoreType.DMA
    vmem = pl.BlockSpec(memory_space=pltpu.VMEM)
    anywhere = pl.BlockSpec(memory_space=pl.ANY)
    return pl.pallas_call(
        functools.partial(kernel, G, S, T, layers, width),
        out_shape=jax.ShapeDtypeStruct((R, F), BF16),
        in_specs=[vmem, vmem, anywhere, vmem, vmem, anywhere, vmem],
        out_specs=vmem,
        scratch_shapes=[
            pltpu.VMEM((layers, width, group), BF16),
            pltpu.VMEM((layers, S, group, w_out.shape[2]), BF16),
            pltpu.VMEM((layers, T, R, F), BF16),
            pltpu.VMEM((layers, T, R, F), BF16),
            pltpu.VMEM((layers, pairs, R, F), BF16),
            pltpu.VMEM((layers, pairs, R, F), BF16),
            pltpu.VMEM((layers, pairs, R, F), BF16),
            pltpu.VMEM((R, F), BF16),
            pltpu.VMEM((R, group), F32),
            pltpu.VMEM((R, 128), F32),
            pltpu.VMEM((R, F), F32),
            pltpu.VMEM((layers, HALO + R, group), BF16),
            pltpu.VMEM((layers, HALO, group), BF16),
            pltpu.VMEM((layers, T, 8, R), F32),
            dma((M,)),
            dma((M, S, 2)),
            dma((M, S)),
            dma((M, S)),
            dma((M, S)),
            dma((layers, pairs, CHUNKS)),
            dma((layers, pairs, CHUNKS)),
            dma((layers, T, CHUNKS)),
            dma((layers, pairs, CHUNKS)),
            dma((layers, pairs, CHUNKS)),
            dma((layers, pairs, CHUNKS)),
            dma((layers, pairs, CHUNKS)),
            dma((layers, T)),
            dma((layers, T)),
            dma((layers,)),
            dma((layers,)),
        ],
        compiler_params=pltpu.CompilerParams(
            collective_id=0, has_side_effects=True, vmem_limit_bytes=60 * 1024 * 1024
        ),
    )(stream, gain_pre, w_in, w_pool, pool_scale, w_out, gain_post)


def solution(mesh):
    G, S, T = mesh.shape["grp"], mesh.shape["sp"], mesh.shape["tp"]
    return jax.shard_map(
        functools.partial(per_device, G, S, T),
        mesh=mesh,
        in_specs=(
            P(("grp", "sp"), "tp"),
            P(),
            P(None, "sp", "tp"),
            P(None, "tp", None, None),
            P(None, "tp"),
            P(None, "tp", "sp"),
            P(),
        ),
        out_specs=P(("grp", "sp"), "tp"),
        check_vma=False,
    )
```

time: 475 us -> 180 us (0.38)
  waiting for transfers between devices: 394 us -> 0 us
  Pallas kernels: 0 us -> 178 us
  matrix products: 22 us -> 0 us
  blocking collectives: 17.3 us -> 0 us
  other arithmetic: 16.3 us -> 0 us
  between operations: 13.7 us -> 0.01 us
  starting transfers between devices: 8.35 us -> 0 us
    all_gather x5 -> x0, waiting for transfers between devices: 295 us -> none  [the longest x1 115 us: per_device(): lax.all_gather(w_in, 'sp', axis=1, tiled=True)]
    pallas_call x0 -> x1, Pallas kernels: none -> 178 us  [per_device(): pl.pallas_call(functools.partial(kernel, G, S, T, layers, width), out_sha...]
    reduce_scatter x3 -> x0, waiting for transfers between devices: 93.6 us -> none  [per_device(): lax.psum_scatter(partial_value, 'tp', scatter_dimension=1, tiled=True)]
    dot_general x6 -> x0, matrix products: 22 us -> none  [the longest x3 13.1 us: per_device(): jnp.dot(mixed, gathered_out[layer], preferred_element_type=jnp.float32)]
    psum x3 -> x0, blocking collectives: 17.3 us -> none  [per_device(): squares = lax.psum(jnp.sum(branch * branch, axis=1), 'tp')]
    reduce_sum x6 -> x0, other arithmetic: 9.92 us -> none  [the longest x3 6.25 us: rms_scale(): inverse = lax.rsqrt(jnp.mean(values * values, axis=-1, keepdims=True) + EPS)]
    ppermute x3 -> x0, starting transfers between devices: 8.07 us -> none  [from_behind(): return lax.ppermute(block, axis, route)]
    convert_element_type x7 -> x0, other arithmetic: 6.38 us -> none  [the longest x3 6.28 us: per_device(): current = (current.astype(jnp.float32) + normed_branch).astype(jnp.bfloat16)]
  transfers between devices with their start and end apart: 11 -> 0, of which waited for: 11 -> 0; matrix products, arithmetic and copies ran while one was open for 1% -> 0% of each run, Pallas kernels for 0% -> 0%
where the time goes in v1:
time: 180 us; the launch traced here: 179 us
  Pallas kernels  178 us (99%)
  local copies, waits for them, and re-layouts  1.87 us (1%)
    pallas_call x1, Pallas kernels, per_device(): pl.pallas_call(functools.partial(kernel, G, S, T, layers, width), out_sha...  178 us

profile of v1, /device:TPU:0, one launch (start us, length us, event | category | flops | bytes accessed | tf_op | source)
XLA Modules:
  0.0 179.4 jit_solution(18274295039702865556)
XLA Ops:
  0.0 177.5 %shard_map.73 = bf16[256,1024]{1,0:T(8,128)(2,1)} custom-call(bf16[256,1024]{1,0:T(8,128)(2,1)} %stream.1, f32[3,4096]{1,0:T(4,128)} %gain_pre.1, bf16[3,1024,256]{2,1,0:T(8,128)(2,1)} %w_in.1, bf16[3,1,256,256]{3,2,1,0:T(8,128)(2,1)} %w_pool.1, f32[3,256]{1,0:T(4,128)} %pool_scale.1, bf16[3,256,1024]{2,1,0:T(8,128)(2,1)} %w_out.1, f32[3,4096]{1,0:T(4,128)} %gain_post.1), custom_call_target="tpu_custom_call" | custom-call | tf_op jit(solution)/shard_map/pallas_call | solution.py:341
  177.5 1.9 %copy.9 = bf16[256,1024]{1,0:T(8,128)(2,1)} copy(bf16[256,1024]{1,0:T(8,128)(2,1)} %shard_map.73) | data formatting | bytes 1048576

commit v2 on v1

v2 whole, which is shorter than its diff:
```python
import functools

import jax
import jax.numpy as jnp
from jax import lax
from jax.experimental import pallas as pl
from jax.experimental.pallas import tpu as pltpu
from jax.sharding import PartitionSpec as P

EPS = 1e-06
HALO = 16
CHUNKS = 4
PIECES = 2
MESH = pl.DeviceIdType.MESH
F32 = jnp.float32
BF16 = jnp.bfloat16


def kernel(
    G, S, T, layers, width,
    stream, gain_pre, w_in, w_pool, pool_scale, w_out, gain_post,
    out,
    win, wout, ag, part, pair, summed, xgot, normed, acc, ss, scale, branch, ext, halo, sq,
    load_sem, zs_sem, zr_sem, ys_sem, yr_sem,
    agp_sem, agx_sem, agr_sem, ps_sem, pr_sem, xs_sem, xr_sem, qs_sem, qr_sem, hs_sem, hr_sem,
):
    g, s, t = lax.axis_index("grp"), lax.axis_index("sp"), lax.axis_index("tp")
    pairs = T // 2
    p, c = lax.div(t, 2), lax.rem(t, 2)
    mate = p * 2 + 1 - c
    R, F = stream.shape
    group = w_pool.shape[2]
    rows_in, cols_out = w_in.shape[1], w_out.shape[2]
    per = S // T
    use_y = G == 2

    def remote(src, dst, send, recv, where):
        return pltpu.make_async_remote_copy(
            src_ref=src, dst_ref=dst, send_sem=send, recv_sem=recv,
            device_id=where, device_id_type=MESH,
        )

    def span(m, src, h):
        size = rows_in if m % 2 == 0 else group
        share = size // 2 if use_y else size
        length = share // PIECES
        start = (g * share if use_y else 0) + h * length
        if m % 2 == 0:
            return win.at[m // 2, pl.ds(pl.multiple_of(src * size + start, 16), length), :]
        return wout.at[m // 2, src, pl.ds(pl.multiple_of(start, 16), length), :]

    def z_copy(m, src, way, h):
        view = span(m, src, h)
        to = s + 1 if way == 0 else s - 1
        return remote(view, view, zs_sem.at[m, src, way, h], zr_sem.at[m, src, h], {"sp": to})

    def y_copy(m, src, h):
        view = span(m, src, h)
        return remote(view, view, ys_sem.at[m, src, h], yr_sem.at[m, src, h], {"grp": 1 - g})

    def load(m):
        if m % 2 == 0:
            return pltpu.make_async_copy(
                w_in.at[m // 2],
                win.at[m // 2, pl.ds(pl.multiple_of(s * rows_in, 16), rows_in), :],
                load_sem.at[m],
            )
        return pltpu.make_async_copy(w_out.at[m // 2], wout.at[m // 2, s], load_sem.at[m])

    M = 2 * layers

    def own(m):
        if m < M:
            load(m).wait()
            for h in range(PIECES):
                pl.when(s < S - 1)(lambda: z_copy(m, s, 0, h).start())
                pl.when(s > 0)(lambda: z_copy(m, s, 1, h).start())

    def relay(m, k, h):
        def from_left():
            src = s - 1 - k
            z_copy(m, src, 0, h).wait_recv()
            pl.when(s < S - 1)(lambda: z_copy(m, src, 0, h).start())
            if use_y:
                y_copy(m, src, h).start()

        def from_right():
            src = s + 1 + k
            z_copy(m, src, 1, h).wait_recv()
            pl.when(s > 0)(lambda: z_copy(m, src, 1, h).start())
            if use_y:
                y_copy(m, src, h).start()

        pl.when(s - 1 - k >= 0)(from_left)
        pl.when(s + 1 + k <= S - 1)(from_right)

    units = [(m, k, h) for m in range(M) for k in range(S - 1) for h in range(PIECES)]
    done = [0]

    def tick(n=1):
        for mm, k, h in units[done[0] : done[0] + n]:
            relay(mm, k, h)
            if k == min(1, S - 2) and h == PIECES - 1:
                own(mm + 1)
            done[0] += 1

    def pump(m):
        tick(max(0, (m + 1) * (S - 1) * PIECES - done[0]))

    def finish(m):
        if use_y:
            for src in range(S):
                for h in range(PIECES):
                    pl.when(s != src)(lambda: y_copy(m, src, h).wait_recv())

    def cut(l):
        return R // 2 - HALO * (layers - 1) + HALO * l

    def span_in(l, a):
        return (cut(l), R) if a == 0 else (0, cut(l))

    def span_out(l, a):
        return span_in(l + 1, a)

    def bits(bounds):
        lo, hi = bounds
        mid = lo + ((hi - lo) // 2 + 15) // 16 * 16
        return [(lo, mid), (mid, hi)]

    def sweep(bounds, body):
        lo, hi = bounds
        step = 32 if (hi - lo) % 32 == 0 else 16

        def one(i, carry):
            body(pl.ds(pl.multiple_of(lo + i * step, 16), step))
            return carry

        lax.fori_loop(0, (hi - lo) // step, one, 0)

    def lanes(x):
        return sum(x[:, i : i + 128] for i in range(0, F, 128))

    def ag_copy(l, block, a, i, sem, to):
        lo, hi = bits(span_in(l, a))[i]
        view = ag.at[l, block, pl.ds(lo, hi - lo), :]
        n = a * 2 + i
        return remote(view, view, sem, agr_sem.at[l, block, n], {"tp": to})

    def ag_start(l, a):
        for i in range(2):
            n = a * 2 + i
            for d in range(1, pairs):
                q = lax.rem(p + d, pairs)
                ag_copy(l, t, a, i, agx_sem.at[l, q, n], q * 2 + c).start()
        for i in range(2):
            ag_copy(l, t, a, i, agp_sem.at[l, p, a * 2 + i], mate).start()

    def ag_wait(l, block, a):
        for i in range(2):
            ag_copy(l, block, a, i, agp_sem.at[l, p, a * 2 + i], mate).wait_recv()

    def ag_relay(l, a):
        for d in range(1, pairs):
            q = lax.rem(p + d, pairs)
            for i in range(2):
                copy = ag_copy(l, q * 2 + c, a, i, agp_sem.at[l, q, a * 2 + i], mate)
                copy.wait_recv()
                copy.start()

    def absorb(l, block, a, first):
        lo, hi = span_in(l, a)
        gain = gain_pre[pl.ds(l, 1), pl.ds(pl.multiple_of(block * F, 128), F)]

        def body(rows):
            x = ag[l, block, rows, :].astype(F32)
            square = lanes(x * x)
            ss[rows, :] = square if first else ss[rows, :] + square
            normed[rows, :] = (x * gain).astype(BF16)

        sweep((lo, hi), body)
        product = jnp.dot(
            normed[lo:hi, :], win[l, pl.ds(pl.multiple_of(block * F, 128), F), :],
            preferred_element_type=F32,
        )
        acc[lo:hi, :] = product if first else acc[lo:hi, :] + product

    def inner(l, a):
        lo, hi = span_in(l, a)
        absorb(l, t, a, True)
        ag_wait(l, mate, a)
        absorb(l, mate, a, False)
        for d in range(1, pairs):
            q = lax.rem(p + d, pairs)
            absorb(l, q * 2 + c, a, False)
            ag_wait(l, q * 2 + 1 - c, a)
            absorb(l, q * 2 + 1 - c, a, False)
        inverse = lax.rsqrt(jnp.sum(ss[lo:hi, :], axis=1, keepdims=True) / width + EPS)
        ext[l, HALO + lo : HALO + hi, :] = (acc[lo:hi, :] * inverse).astype(BF16)

    def halo_copy(l):
        return remote(
            ext.at[l, pl.ds(R, HALO), :], halo.at[l], hs_sem.at[l], hr_sem.at[l], {"sp": s + 1}
        )

    def halo_in(l):
        pl.when(s > 0)(lambda: halo_copy(l).wait_recv())

        @pl.when(s == 0)
        def _():
            ext[l, pl.ds(0, HALO), :] = jnp.zeros((HALO, group), BF16)

        @pl.when(s > 0)
        def _():
            ext[l, pl.ds(0, HALO), :] = halo[l]

    def pool(l, a):
        lo, hi = span_out(l, a)
        values = ext[l, lo : hi + HALO, :].astype(F32)
        two = values + pltpu.roll(values, 1, 0)
        four = two + pltpu.roll(two, 2, 0)
        eight = four + pltpu.roll(four, 4, 0)
        sixteen = eight + pltpu.roll(eight, 8, 0)
        total = jnp.where(t == 0, two, jnp.where(t == 1, four, jnp.where(t == 2, eight, sixteen)))
        window = jnp.where(t == 0, 2, jnp.where(t == 1, 4, jnp.where(t == 2, 8, 16)))
        place = s * R + lo + lax.broadcasted_iota(jnp.int32, (hi - lo, group), 0)
        count = jnp.minimum(place + 1, window).astype(F32)
        spread = (total[HALO:, :] / count - values[HALO:, :]).astype(BF16)
        mixed = jnp.dot(spread, w_pool[l, 0], preferred_element_type=F32)
        return (mixed * pool_scale[l : l + 1, :]).astype(BF16)

    def project(l, a, dest, mixed):
        lo, hi = span_out(l, a)
        for k in range(per):
            value = jnp.dot(mixed, wout[l, dest * per + k], preferred_element_type=F32)
            part[l, dest, lo:hi, k * cols_out : (k + 1) * cols_out] = value.astype(BF16)

    def pair_copy(l, q, a, i):
        lo, hi = bits(span_out(l, a))[i]
        rows, n = pl.ds(lo, hi - lo), a * 2 + i
        return remote(
            part.at[l, q * 2 + 1 - c, rows, :], pair.at[l, q, rows, :],
            ps_sem.at[l, q, n], pr_sem.at[l, q, n], {"tp": mate},
        )

    def cross_copy(l, q, slot, a, i):
        lo, hi = bits(span_out(l, a))[i]
        rows, n = pl.ds(lo, hi - lo), a * 2 + i
        return remote(
            summed.at[l, q, rows, :], xgot.at[l, slot, rows, :],
            xs_sem.at[l, q, n], xr_sem.at[l, slot, n], {"tp": q * 2 + c},
        )

    def scatter_first(l, a, mixed):
        for d in range(1, pairs):
            q = lax.rem(p + d, pairs)
            project(l, a, q * 2 + 1 - c, mixed)
            for i in range(2):
                pair_copy(l, q, a, i).start()
        for d in range(1, pairs):
            project(l, a, lax.rem(p + d, pairs) * 2 + c, mixed)

    def scatter_cross(l, a):
        for d in range(1, pairs):
            q = lax.rem(p + d, pairs)
            for i in range(2):
                pair_copy(l, q, a, i).wait_recv()

                def body(rows):
                    summed[l, q, rows, :] = (
                        part[l, q * 2 + c, rows, :].astype(F32) + pair[l, q, rows, :].astype(F32)
                    ).astype(BF16)

                sweep(bits(span_out(l, a))[i], body)
                cross_copy(l, q, p, a, i).start()

    def scatter_own(l, a, mixed):
        project(l, a, mate, mixed)
        for i in range(2):
            pair_copy(l, p, a, i).start()
        project(l, a, t, mixed)

    def sq_copy(l, slot, a, to):
        view = sq.at[l, a, slot]
        return remote(view, view, qs_sem.at[l, a, to], qr_sem.at[l, a, slot], {"tp": to})

    def settle(l, a):
        for i in range(2):
            pair_copy(l, p, a, i).wait_recv()
            for d in range(1, pairs):
                q = lax.rem(p + d, pairs)
                cross_copy(l, q, q, a, i).wait_recv()

            def add(rows):
                value = part[l, t, rows, :].astype(F32) + pair[l, p, rows, :].astype(F32)
                for d in range(1, pairs):
                    value = value + xgot[l, lax.rem(p + d, pairs), rows, :].astype(F32)
                branch[rows, :] = value
                ss[rows, :] = lanes(value * value)

            sweep(bits(span_out(l, a))[i], add)
        row = jnp.sum(jnp.transpose(ss[...]), axis=0, keepdims=True)
        sq[l, a, t] = jnp.broadcast_to(row, (8, R))
        for d in range(1, T):
            sq_copy(l, t, a, lax.rem(t + d, T)).start()
        tick()
        for d in range(1, T):
            other = lax.rem(t + d, T)
            sq_copy(l, other, a, other).wait_recv()
        squares = sq[l, a, 0]
        for k in range(1, T):
            squares = squares + sq[l, a, k]
        inverse = lax.rsqrt(squares / width + EPS)
        scale[...] = jnp.transpose(jnp.concatenate([inverse] * 16, axis=0))
        gain = gain_post[pl.ds(l, 1), pl.ds(pl.multiple_of(t * F, 128), F)]

        def update(rows):
            value = ag[l, t, rows, :].astype(F32) + branch[rows, :] * scale[rows, 0:1] * gain
            if l + 1 < layers:
                ag[l + 1, t, rows, :] = value.astype(BF16)
            else:
                out[rows, :] = value.astype(BF16)

        sweep(span_out(l, a), update)
        if l + 1 < layers:
            ag_start(l + 1, a)

    for m in range(M):
        load(m).start()
    barrier = pltpu.get_barrier_semaphore()

    def greet(where):
        pl.semaphore_signal(barrier, inc=1, device_id=where, device_id_type=MESH)

    pl.when(s < S - 1)(lambda: greet({"sp": s + 1}))
    pl.when(s > 0)(lambda: greet({"sp": s - 1}))
    if use_y:
        greet({"grp": 1 - g})
    for d in range(1, T):
        greet({"tp": lax.rem(t + d, T)})
    ag[0, t] = stream[...]
    ends = jnp.where(s > 0, 1, 0) + jnp.where(s < S - 1, 1, 0)
    pl.semaphore_wait(barrier, ends + (1 if use_y else 0) + T - 1)

    own(0)
    ag_start(0, 0)
    ag_start(0, 1)
    each = (S - 1) * PIECES
    for l in range(layers):
        if l == 0:
            tick(each // 3)
            ag_relay(0, 0)
            tick(each // 3)
            ag_relay(0, 1)
        else:
            ag_relay(l, 0)
        pump(2 * l)
        finish(2 * l)
        inner(l, 0)
        pl.when(s < S - 1)(lambda: halo_copy(l).start())
        mixed = pool(l, 0)
        if l == 0:
            tick()
            inner(l, 1)
            tick()
            halo_in(l)
            later = pool(l, 1)
        pump(2 * l + 1)
        finish(2 * l + 1)
        scatter_first(l, 0, mixed)
        tick()
        if l > 0:
            ag_relay(l, 1)
        scatter_cross(l, 0)
        tick()
        scatter_own(l, 0, mixed)
        tick()
        if l > 0:
            inner(l, 1)
            tick()
            halo_in(l)
            later = pool(l, 1)
        scatter_first(l, 1, later)
        tick()
        scatter_cross(l, 1)
        tick()
        scatter_own(l, 1, later)
        tick()
        settle(l, 0)
        tick()
        settle(l, 1)
        tick()

    for l in range(layers):
        pl.when(s < S - 1)(lambda: halo_copy(l).wait_send())
        for a in range(2):
            for d in range(1, T):
                sq_copy(l, t, a, lax.rem(t + d, T)).wait_send()
            for i in range(2):
                n = a * 2 + i
                for q in range(pairs):
                    ag_copy(l, t, a, i, agp_sem.at[l, q, n], mate).wait_send()
                    pair_copy(l, q, a, i).wait_send()
                for d in range(1, pairs):
                    q = lax.rem(p + d, pairs)
                    ag_copy(l, t, a, i, agx_sem.at[l, q, n], mate).wait_send()
                    cross_copy(l, q, p, a, i).wait_send()
    for m in range(M):
        for src in range(S):
            for h in range(PIECES):
                pl.when(jnp.logical_and(src <= s, s < S - 1))(lambda: z_copy(m, src, 0, h).wait_send())
                pl.when(jnp.logical_and(src >= s, s > 0))(lambda: z_copy(m, src, 1, h).wait_send())
                if use_y:
                    pl.when(s != src)(lambda: y_copy(m, src, h).wait_send())


def per_device(G, S, T, stream, gain_pre, w_in, w_pool, pool_scale, w_out, gain_post):
    layers, width = gain_pre.shape
    R, F = stream.shape
    group = w_pool.shape[2]
    pairs = T // 2
    M = 2 * layers
    dma = pltpu.SemaphoreType.DMA
    vmem = pl.BlockSpec(memory_space=pltpu.VMEM)
    anywhere = pl.BlockSpec(memory_space=pl.ANY)
    return pl.pallas_call(
        functools.partial(kernel, G, S, T, layers, width),
        out_shape=jax.ShapeDtypeStruct((R, F), BF16),
        in_specs=[vmem, vmem, anywhere, vmem, vmem, anywhere, vmem],
        out_specs=vmem,
        scratch_shapes=[
            pltpu.VMEM((layers, width, group), BF16),
            pltpu.VMEM((layers, S, group, w_out.shape[2]), BF16),
            pltpu.VMEM((layers, T, R, F), BF16),
            pltpu.VMEM((layers, T, R, F), BF16),
            pltpu.VMEM((layers, pairs, R, F), BF16),
            pltpu.VMEM((layers, pairs, R, F), BF16),
            pltpu.VMEM((layers, pairs, R, F), BF16),
            pltpu.VMEM((R, F), BF16),
            pltpu.VMEM((R, group), F32),
            pltpu.VMEM((R, 128), F32),
            pltpu.VMEM((R, 128), F32),
            pltpu.VMEM((R, F), F32),
            pltpu.VMEM((layers, HALO + R, group), BF16),
            pltpu.VMEM((layers, HALO, group), BF16),
            pltpu.VMEM((layers, 2, T, 8, R), F32),
            dma((M,)),
            dma((M, S, 2, PIECES)),
            dma((M, S, PIECES)),
            dma((M, S, PIECES)),
            dma((M, S, PIECES)),
            dma((layers, pairs, CHUNKS)),
            dma((layers, pairs, CHUNKS)),
            dma((layers, T, CHUNKS)),
            dma((layers, pairs, CHUNKS)),
            dma((layers, pairs, CHUNKS)),
            dma((layers, pairs, CHUNKS)),
            dma((layers, pairs, CHUNKS)),
            dma((layers, 2, T)),
            dma((layers, 2, T)),
            dma((layers,)),
            dma((layers,)),
        ],
        compiler_params=pltpu.CompilerParams(
            collective_id=0, has_side_effects=True, vmem_limit_bytes=60 * 1024 * 1024
        ),
    )(stream, gain_pre, w_in, w_pool, pool_scale, w_out, gain_post)


def solution(mesh):
    G, S, T = mesh.shape["grp"], mesh.shape["sp"], mesh.shape["tp"]
    return jax.shard_map(
        functools.partial(per_device, G, S, T),
        mesh=mesh,
        in_specs=(
            P(("grp", "sp"), "tp"),
            P(),
            P(None, "sp", "tp"),
            P(None, "tp", None, None),
            P(None, "tp"),
            P(None, "tp", "sp"),
            P(),
        ),
        out_specs=P(("grp", "sp"), "tp"),
        check_vma=False,
    )
```

time: 180 us -> 146 us (0.81)
  Pallas kernels: 178 us -> 144 us
    pallas_call x1, Pallas kernels: 178 us -> 144 us  [per_device(): pl.pallas_call(functools.partial(kernel, G, S, T, layers, width), out_sha...]
where the time goes in v2:
time: 146 us
  Pallas kernels  144 us (99%)
  local copies, waits for them, and re-layouts  1.87 us (1%)
    pallas_call x1, Pallas kernels, per_device(): pl.pallas_call(functools.partial(kernel, G, S, T, layers, width), out_sha...  144 us

profile of v2, /device:TPU:0, one launch (start us, length us, event | category | flops | bytes accessed | tf_op | source)
XLA Modules:
  0.0 145.6 jit_solution(13568392885194236190)
XLA Ops:
  0.0 143.7 %shard_map.73 = bf16[256,1024]{1,0:T(8,128)(2,1)} custom-call(bf16[256,1024]{1,0:T(8,128)(2,1)} %stream.1, f32[3,4096]{1,0:T(4,128)} %gain_pre.1, bf16[3,1024,256]{2,1,0:T(8,128)(2,1)} %w_in.1, bf16[3,1,256,256]{3,2,1,0:T(8,128)(2,1)} %w_pool.1, f32[3,256]{1,0:T(4,128)} %pool_scale.1, bf16[3,256,1024]{2,1,0:T(8,128)(2,1)} %w_out.1, f32[3,4096]{1,0:T(4,128)} %gain_post.1), custom_call_target="tpu_custom_call" | custom-call | tf_op jit(solution)/shard_map/pallas_call | solution.py:425
  143.7 1.9 %copy.9 = bf16[256,1024]{1,0:T(8,128)(2,1)} copy(bf16[256,1024]{1,0:T(8,128)(2,1)} %shard_map.73) | data formatting | bytes 1048576
